TPU v7x, 512 devices: a whole 4x8x8 slice. The times are simulated.
512 devices in a mesh: sp: 64 (over z, y), tp: 8 (over x, core).
Axes of the slice: x: 4, y: 8, z: 8, core: 2. Of those that a mesh axis runs over, the one named last changes fastest.
Arguments:
- inputs: bfloat16 [24576, 2048], P(('sp', 'tp')), may hold values from -6 to 6
- norm_gain: float32 [2048], replicated, may hold values from 0.1 to 1.9
- latent_down: bfloat16 [2048, 256], P('sp'), may hold values from -0.125 to 0.125
- rope_down: bfloat16 [2048, 64], P('sp'), may hold values from -0.125 to 0.125
- latent_gain: float32 [256], replicated, may hold values from 0.1 to 1.9
- mla_query: bfloat16 [2048, 1536], P(None, 'tp'), as said below
- key_up: bfloat16 [256, 1024], replicated, may hold values from -3.5 to 3.5
- value_up: bfloat16 [256, 1024], replicated, may hold values from -1.75 to 1.75
- swa_query: bfloat16 [2048, 1024], P(None, 'tp'), as said below
- swa_key: bfloat16 [2048, 512], P(None, 'tp'), may hold values from -0.125 to 0.125
- swa_value: bfloat16 [2048, 512], P(None, 'tp'), may hold values from -0.125 to 0.125
- sink_logits: float32 [16], replicated, may hold values from 1 to 6
- out_mla: bfloat16 [1024, 2048], P(None, 'tp'), may hold values from -0.875 to 0.875
- out_swa: bfloat16 [1024, 2048], P(None, 'tp'), may hold values from -0.875 to 0.875
Outputs:
- mixed: bfloat16 [24576, 2048], P('sp', 'tp')
Inputs may be any that keep to these rules, and one draw needn't show every extreme that they name: `mla_query`: entries lie within 360 / sqrt(2048) in magnitude. `swa_query`: entries lie within 900 / sqrt(2048) in magnitude.
All inputs are finite; a program needn't handle non-finite values.
Results may differ from a plain program's by a relative error of at most 0.02.
The roundings to bfloat16 on the way count: a program that leaves them out, or rounds other values in their place, can miss the bound.
Values may be sent and summed in bfloat16 or wider, within the bound.
No kernel may reach another device: no remote copies, remote signals or barrier semaphores. Data moves between devices by JAX's collectives and lax.ppermute only.
A program may use at most 64 MiB of HBM per device.

v0:
```python
import math
import jax
import jax.numpy as jnp
from jax import lax
from jax.sharding import Mesh
from jax.sharding import PartitionSpec as P

NOPE = 128
ROPE = 64
VDIM = 128
KV_RANK = 256
HEAD = 64
WINDOW = 128
SP = ("sp_0", "sp_1")
SP_TP = ("sp_0", "sp_1", "tp")
NORM_EPS = 1e-06
ROPE_BASE = 10000.0
MASKED_VALUE = -1e30
KEY_SPAN = 512


def joined_along(tiles, dim):
    tiles = jnp.moveaxis(tiles, 0, dim)
    lengths = tiles.shape
    return tiles.reshape(*lengths[:dim], lengths[dim] * lengths[dim + 1], *lengths[dim + 2 :])


def copy_for_each(array, axis):
    copies = jnp.broadcast_to(array, (lax.axis_size(axis), *array.shape))
    return lax.all_to_all(copies, axis, split_axis=0, concat_axis=0, tiled=True)


def gathered_copies(array, axis, dim):
    return joined_along(copy_for_each(array, axis), dim)


def in_one_piece(arrays, axis, dim, along):
    ends, at = ([], 0)
    for a in arrays[:-1]:
        at += a.shape[along]
        ends.append(at)
    both = jnp.concatenate(arrays, axis=along)
    return tuple(jnp.split(lax.all_gather(both, axis, axis=dim, tiled=True), ends, axis=along))


def stacked_from(array, axes, turns):
    tiles = array[None]
    for k in turns:
        tiles = lax.all_gather(tiles, axes[k], axis=0, tiled=True)
    held = [lax.axis_size(axes[k]) for k in reversed(turns)]
    tiles = tiles.reshape(*held, *array.shape)
    turned = sorted(range(len(turns)), key=lambda place: turns[len(turns) - 1 - place])
    return tiles.transpose(*turned, *range(len(turns), tiles.ndim)).reshape(-1, *array.shape)


def gather_axes(array, axes, turns, dim):
    return joined_along(stacked_from(array, axes, turns), dim)


def of_everyone(array, axis):
    everything = copy_for_each(array, axis)
    return jnp.max(everything, axis=0)


def in_one_piece_2(arrays, axis, dim, along):
    widths = [math.prod(a.shape[along:]) for a in arrays]
    both = jnp.concatenate(
        [a.reshape(*a.shape[:along], w) for a, w in zip(arrays, widths)], axis=along
    )
    result = lax.psum_scatter(both, axis, scatter_dimension=dim, tiled=True)
    tiles = jnp.split(result, [sum(widths[:k]) for k in range(1, len(widths))], axis=along)
    return tuple(
        (b.reshape(*result.shape[:along], *a.shape[along:]) for a, b in zip(arrays, tiles))
    )


def from_behind(value, axis, steps):
    count = lax.axis_size(axis)
    first, last = (max(0, -steps), min(count, count - steps))
    return lax.ppermute(value, axis, [(source, source + steps) for source in range(first, last)])


def to_float(values):
    return lax.optimization_barrier(values).astype(jnp.float32)


def norm_rows(values, gains):
    widened = to_float(values)
    scaled = widened * lax.rsqrt(jnp.mean(widened * widened, axis=-1, keepdims=True) + NORM_EPS)
    return (scaled * gains).astype(jnp.bfloat16)


def rotate(values, positions):
    full_width = values.shape[-1]
    half_width = full_width // 2
    inverse = ROPE_BASE ** (-jnp.arange(0, full_width, 2, dtype=jnp.float32) / full_width)
    angles = positions.astype(jnp.float32)[:, None] * inverse[None, :]
    shaped = (values.shape[0],) + (1,) * (values.ndim - 2) + (half_width,)
    cos_table = jnp.cos(angles).reshape(shaped)
    sin_table = jnp.sin(angles).reshape(shaped)
    widened = to_float(values)
    first_half = widened[..., :half_width]
    second_half = widened[..., half_width:]
    return jnp.concatenate(
        [
            first_half * cos_table - second_half * sin_table,
            first_half * sin_table + second_half * cos_table,
        ],
        axis=-1,
    ).astype(jnp.bfloat16)


def attend_latent(
    state_in, keys_latent, keys_rope, key_positions, query_latent, query_rope, query_pos, mla_scale
):
    key_count = keys_latent.shape[0]
    span_rows = math.gcd(key_count, KEY_SPAN)
    last_query = query_pos[-1]

    def update(step_index, state):
        span_pos = lax.dynamic_slice_in_dim(key_positions, step_index * span_rows, span_rows, 0)

        def compute(current):
            running_max, denom_sum, weighted = current
            lat_block = lax.dynamic_slice_in_dim(keys_latent, step_index * span_rows, span_rows, 0)
            rope_block = lax.dynamic_slice_in_dim(keys_rope, step_index * span_rows, span_rows, 0)
            scores = (
                jnp.einsum(
                    "htj,sj->hts", query_latent, lat_block, preferred_element_type=jnp.float32
                )
                + jnp.einsum(
                    "htd,sd->hts", query_rope, rope_block, preferred_element_type=jnp.float32
                )
            ) * mla_scale
            allowed = span_pos[None, None, :] <= query_pos[None, :, None]
            scores = jnp.where(allowed, scores, MASKED_VALUE)
            new_max = jnp.maximum(running_max, jnp.max(scores, axis=-1))
            weights_raw = jnp.where(allowed, jnp.exp(scores - new_max[..., None]), 0.0)
            rescale = jnp.exp(running_max - new_max)
            denom_sum = denom_sum * rescale + jnp.sum(weights_raw, axis=-1)
            weighted = weighted * rescale[..., None] + jnp.einsum(
                "hts,sj->htj",
                weights_raw.astype(jnp.bfloat16),
                lat_block,
                preferred_element_type=jnp.float32,
            )
            return (new_max, denom_sum, weighted)

        return lax.cond(span_pos[0] <= last_query, compute, lambda current: current, state)

    return lax.fori_loop(0, key_count // span_rows, update, state_in)


def shards(
    inputs,
    norm_gain,
    latent_down,
    rope_down,
    latent_gain,
    mla_query,
    key_up,
    value_up,
    swa_query,
    swa_key,
    swa_value,
    sink_logits,
    out_mla,
    out_swa,
):
    own_rows = inputs.shape[0]
    tp_count = lax.axis_size("tp")
    block_rows = own_rows * tp_count
    tp_rank = lax.axis_index("tp")
    offset = lax.axis_index(SP) * block_rows
    own_pos = offset + tp_rank * own_rows + jnp.arange(own_rows, dtype=jnp.int32)
    block_pos = offset + jnp.arange(block_rows, dtype=jnp.int32)
    width_mla = mla_query.shape[1]
    width_swa = swa_query.shape[1]
    width_kv = swa_key.shape[1]
    heads_mla = width_mla // (NOPE + ROPE)
    heads_swa = width_swa // HEAD
    groups_kv = width_kv // HEAD
    group = heads_swa // groups_kv
    normed = norm_rows(inputs, norm_gain)
    pieces = gathered_copies(normed, "tp", 0)
    projected = jnp.concatenate(
        [
            jnp.dot(pieces, mla_query, preferred_element_type=jnp.float32).astype(jnp.bfloat16),
            jnp.dot(pieces, swa_query, preferred_element_type=jnp.float32).astype(jnp.bfloat16),
            jnp.dot(pieces, swa_key, preferred_element_type=jnp.float32).astype(jnp.bfloat16),
            jnp.dot(pieces, swa_value, preferred_element_type=jnp.float32).astype(jnp.bfloat16),
        ],
        axis=1,
    )
    pieces = in_one_piece((latent_down, rope_down), SP, 0, 1)
    latent = jnp.dot(normed, pieces[0], preferred_element_type=jnp.float32)
    rope_raw = jnp.dot(normed, pieces[1], preferred_element_type=jnp.float32)
    keys_latent = norm_rows(latent.astype(jnp.bfloat16), latent_gain)
    keys_rope = rotate(rope_raw.astype(jnp.bfloat16), own_pos)
    queries = projected[:, :width_mla].reshape(block_rows, heads_mla, NOPE + ROPE)
    query_rope = jnp.transpose(rotate(queries[:, :, NOPE:], block_pos), (1, 0, 2))
    head_first = tp_rank * heads_mla
    up_keys = lax.dynamic_slice_in_dim(key_up, head_first * NOPE, heads_mla * NOPE, 1)
    up_keys = up_keys.reshape(KV_RANK, heads_mla, NOPE)
    query_latent = jnp.einsum(
        "thn,jhn->htj", queries[:, :, :NOPE], up_keys, preferred_element_type=jnp.float32
    ).astype(jnp.bfloat16)
    mla_scale = (NOPE + ROPE) ** (-0.5)
    every_latent, every_rope = in_one_piece((query_latent, query_rope), "tp", 0, 2)
    slice_latent, slice_rope = (
        gather_axes(keys_latent, SP, (0, 1), 0),
        gather_axes(keys_rope, SP, (0, 1), 0),
    )
    heads_all = every_latent.shape[0]
    row_index = jnp.arange(slice_latent.shape[0], dtype=jnp.int32)
    slice_pos = row_index // own_rows * block_rows + tp_rank * own_rows + row_index % own_rows
    slice_state = (
        jnp.full((heads_all, block_rows), MASKED_VALUE, jnp.float32),
        jnp.zeros((heads_all, block_rows), jnp.float32),
        jnp.zeros((heads_all, block_rows, KV_RANK), jnp.float32),
    )
    part_max, part_sum, part_weighted = attend_latent(
        slice_state,
        slice_latent,
        slice_rope,
        slice_pos,
        every_latent,
        every_rope,
        block_pos,
        mla_scale,
    )
    global_max = of_everyone(part_max, "tp")
    rescale = jnp.exp(part_max - global_max)
    denom_sum, weighted = tuple(
        (
            part.astype(jnp.float32)
            for part in in_one_piece_2(
                (
                    (part_sum * rescale).astype(jnp.bfloat16),
                    (part_weighted * rescale[..., None]).astype(jnp.bfloat16),
                ),
                "tp",
                0,
                2,
            )
        )
    )
    latent_out = (weighted / denom_sum[..., None]).astype(jnp.bfloat16)
    up_values = lax.dynamic_slice_in_dim(value_up, head_first * VDIM, heads_mla * VDIM, 1)
    up_values = up_values.reshape(KV_RANK, heads_mla, VDIM)
    mla_out = jnp.einsum(
        "htj,jhv->thv", latent_out, up_values, preferred_element_type=jnp.float32
    ).astype(jnp.bfloat16)
    mla_out = mla_out.reshape(block_rows, heads_mla * VDIM)
    swa_q = projected[:, width_mla : width_mla + width_swa].reshape(
        block_rows, groups_kv, group, HEAD
    )
    swa_k = projected[:, width_mla + width_swa : width_mla + width_swa + width_kv]
    swa_v = projected[:, width_mla + width_swa + width_kv : width_mla + width_swa + 2 * width_kv]
    prev_keys, prev_values = from_behind(
        (swa_k[block_rows - WINDOW :], swa_v[block_rows - WINDOW :]), SP, 1
    )
    window_keys_all = jnp.concatenate([prev_keys, swa_k], axis=0).reshape(
        WINDOW + block_rows, groups_kv, HEAD
    )
    window_values = jnp.concatenate([prev_values, swa_v], axis=0).reshape(
        WINDOW + block_rows, groups_kv, HEAD
    )
    scores = jnp.einsum(
        "tkgd,skd->kgts", swa_q, window_keys_all, preferred_element_type=jnp.float32
    ) * HEAD ** (-0.5)
    key_pos = offset - WINDOW + jnp.arange(WINDOW + block_rows, dtype=jnp.int32)
    distance = block_pos[:, None] - key_pos[None, :]
    allowed = (distance >= 0) & (distance < WINDOW) & (key_pos[None, :] >= 0)
    scores = jnp.where(allowed, scores, MASKED_VALUE)
    sink_table = lax.dynamic_slice_in_dim(sink_logits, tp_rank * heads_swa, heads_swa, 0)
    sink_table = sink_table.reshape(groups_kv, group, 1, 1)
    row_max = jnp.maximum(jnp.max(scores, axis=-1, keepdims=True), sink_table)
    weights_raw = jnp.exp(scores - row_max)
    weights = (
        weights_raw / (jnp.sum(weights_raw, axis=-1, keepdims=True) + jnp.exp(sink_table - row_max))
    ).astype(jnp.bfloat16)
    swa_out = jnp.einsum(
        "kgts,skd->tkgd", weights, window_values, preferred_element_type=jnp.float32
    ).astype(jnp.bfloat16)
    swa_out = swa_out.reshape(block_rows, heads_swa * HEAD)
    all_mla, all_swa = in_one_piece((mla_out, swa_out), "tp", 1, 0)
    mixed = jnp.dot(all_mla, out_mla, preferred_element_type=jnp.float32) + jnp.dot(
        all_swa, out_swa, preferred_element_type=jnp.float32
    )
    return mixed.astype(jnp.bfloat16)


def solution(mesh):
    split = Mesh(mesh.devices.reshape(8, 8, mesh.shape["tp"]), ("sp_0", "sp_1", "tp"))
    placed = (
        P(SP_TP, None),
        P(),
        P(SP, None),
        P(SP, None),
        P(),
        P(None, "tp"),
        P(),
        P(),
        P(None, "tp"),
        P(None, "tp"),
        P(None, "tp"),
        P(),
        P(None, "tp"),
        P(None, "tp"),
    )
    return jax.shard_map(
        shards, mesh=split, in_specs=placed, out_specs=P(SP, "tp"), check_vma=False
    )
```

profile of v0, /device:TPU:1, one launch (start us, length us, event | category | flops | bytes accessed | tf_op | source)
XLA Modules:
  0.0 359.5 jit_solution(10568069677121225495)
XLA Ops:
  6.5 1.4 pad_maximum_fusion.3
  10.1 1.4 broadcast_in_dim.68
  11.5 10.3 %all-to-all-start = ((bf16[8,48,2048]{2,1,0:T(8,128)(2,1)}), bf16[8,48,2048]{2,1,0:T(8,128)(2,1)S(1)}, u32[]{:S(2)}, u32[]{:S(2)}) async-start(bf16[8,48,2048]{2,1,0:T(8,128)(2,1)} %broadcast_in_dim.68), calls=%async_computation | async-start | bytes 3145728 | tf_op jit(solution)/shard_map/all_to_all | solution.py:30
  21.8 20.6 %all-to-all-done = bf16[8,48,2048]{2,1,0:T(8,128)(2,1)S(1)} async-done(((bf16[8,48,2048]{2,1,0:T(8,128)(2,1)}), bf16[8,48,2048]{2,1,0:T(8,128)(2,1)S(1)}, u32[]{:S(2)}, u32[]{:S(2)}) %all-to-all-start) | async-done | bytes 1572896 | tf_op jit(solution)/shard_map/all_to_all | solution.py:30
  45.3 48.9 %all-gather.6.cloned.1.call-done = bf16[2048,320]{1,0:T(8,128)(2,1)} async-done(((bf16[32,320]{1,0:T(8,128)(2,1)}), bf16[2048,320]{1,0:T(8,128)(2,1)}) %all-gather.6.cloned.1.call-update) | async-done | bytes 1310736 | tf_op jit(solution)/shard_map/all_gather | solution.py:43
  94.2 1.5 convolution_convert_fusion.7
  95.9 20.3 %all-gather = bf16[384,256]{1,0:T(8,128)(2,1)} all-gather(bf16[48,256]{1,0:T(8,128)(2,1)S(1)} %fusion.52), channel_id=2, replica_groups=mesh['sp_0'=8,'sp_1'=8,'tp'=8] {'sp_0'}, dimensions={0}, use_global_device_ids=true | all-gather | bytes 221184 | tf_op jit(solution)/shard_map/all_gather | solution.py:49
  117.0 1.3 convolution_convert_fusion.8
  118.6 18.9 %all_gather.25 = bf16[8,48,64]{2,1,0:T(8,128)(2,1)S(1)} all-gather(bf16[1,48,64]{2,1,0:T(8,128)(2,1)S(1)} %pad_maximum_fusion.4), channel_id=1, replica_groups=mesh['sp_0'=8,'sp_1'=8,'tp'=8] {'sp_0'}, dimensions={0}, use_global_device_ids=true | all-gather | bytes 55296 | tf_op jit(solution)/shard_map/all_gather | solution.py:49
  137.5 23.1 %all_gather.26 = bf16[64,48,64]{2,1,0:T(8,128)(2,1)S(1)} all-gather(bf16[8,48,64]{2,1,0:T(8,128)(2,1)S(1)} %all_gather.25), channel_id=1, replica_groups=mesh['sp_0'=8,'sp_1'=8,'tp'=8] {'sp_1'}, dimensions={0}, use_global_device_ids=true | all-gather | bytes 442368 | tf_op jit(solution)/shard_map/all_gather | solution.py:49
  160.5 1.6 copy.34
  162.2 2.0 reshape_reshape.7
  164.2 2.7 split.33
  166.9 1.7 copy.35
  169.7 2.7 copy.33
  172.5 1.9 broadcast_in_dim.66
  174.4 22.4 %while.18 = (s32[]{:T(128)}, f32[8,384]{1,0:T(8,128)S(1)}, f32[8,384]{1,0:T(8,128)S(1)}, f32[8,384,256]{2,1,0:T(8,128)}, s32[3072]{0:T(1024)S(1)}, /*index=5*/s3...) while((s32[]{:T(128)}, f32[8,384]{1,0:T(8,128)S(1)}, ...), condition=%wide.region_7.8_spmd.clone, body=%wide.region_2.7_spmd.clone.sunk | while | flops 1829443968 | bytes 66466276 | solution.py:151
  176.4 10.4 %conditional.3 = ((f32[8,384]{1,0:T(8,128)S(1)}, f32[8,384]{1,0:T(8,128)S(1)}, f32[8,384,256]{2,1,0:T(8,128)})) conditional(s32[]{:T(128)} %convert_element_type.210, (f32[8,384]{1,0:T(8,128)S(1)}, f32[8,384]{1,0:T(8,128)S(1)}, f32[8,384,256]{2,1,0:T(8,128)}) %tuple.52, (s32[512]{0:T(512)S(1)}, s32[]{:T(128)}, s32[]{:T(128)}, ...), branch_computations={%region_3.3_spmd, %region_4.6_spmd} | conditional | flops 1829443968 | bytes 66460312 | solution.py:149
  177.6 2.5 fusion.85
  180.2 1.1 fusion.3
  182.0 3.1 multiply_add_fusion
  185.1 1.6 copy-done.2
  196.8 29.9 %all_to_all.10 = f32[8,8,384]{2,1,0:T(8,128)S(1)} all-to-all(f32[8,8,384]{2,1,0:T(8,128)S(1)} %broadcast_in_dim.69), channel_id=1, replica_groups=mesh['sp_0'=8,'sp_1'=8,'tp'=8] {'tp'}, dimensions={0} | all-to-all | bytes 196608 | tf_op jit(solution)/shard_map/all_to_all | solution.py:30
  227.2 2.4 multiply_convert_fusion
  229.5 2.5 pad_maximum_fusion
  234.1 2.6 collective-permute-start.1
  237.4 3.1 collective-permute-start
  242.4 73.9 %reduce-scatter.2.cloned.1.call-done = bf16[1,384,257]{2,1,0:T(8,128)(2,1)} async-done(((bf16[8,384,257]{2,1,0:T(8,128)(2,1)}), bf16[1,384,257]{2,1,0:T(8,128)(2,1)}) %reduce-scatter.2.cloned.1.call-update) | async-done | bytes 197392 | tf_op jit(solution)/shard_map/reduce_scatter | solution.py:70
  317.3 1.3 fusion.26
  319.3 30.9 %all-gather.12.cloned.1.call-done = bf16[768,1024]{0,1:T(8,128)(2,1)} async-done(((bf16[768,128]{0,1:T(8,128)(2,1)}), bf16[768,1024]{0,1:T(8,128)(2,1)}) %all-gather.12.cloned.1.call-update) | async-done | bytes 1572880 | tf_op jit(solution)/shard_map/all_gather | solution.py:43
  350.2 1.7 fusion.29
  351.9 1.1 fusion.23
  (112 shorter events, 19.6 us)
Async XLA Ops:
  6.5 35.9 %copy-start = (bf16[2048,192]{0,1:T(8,128)(2,1)S(1)}, bf16[2048,192]{0,1:T(8,128)(2,1)}, u32[]{:S(2)}) copy-start(bf16[2048,192]{0,1:T(8,128)(2,1)} %param.23) | copy-start | bytes 2359300
  6.5 87.7 %all-gather.6.cloned.1.call-start = ((), (), s32[]{:S(2)}) async-start(), calls=%async_computation.3 | async-start | bytes 1597440 | tf_op jit(solution)/shard_map/all_gather | solution.py:43
  11.5 30.9 %all-to-all-start = ((bf16[8,48,2048]{2,1,0:T(8,128)(2,1)}), bf16[8,48,2048]{2,1,0:T(8,128)(2,1)S(1)}, u32[]{:S(2)}, u32[]{:S(2)}) async-start(bf16[8,48,2048]{2,1,0:T(8,128)(2,1)} %broadcast_in_dim.68), calls=%async_computation | async-start | bytes 3145728 | tf_op jit(solution)/shard_map/all_to_all | solution.py:30
  21.8 142.4 %all-gather.10.cloned.1.call-start = ((), (), s32[]{:S(2)}) async-start(), calls=%async_computation.5 | async-start | bytes 2211840 | tf_op jit(solution)/shard_map/all_gather | solution.py:43
  42.4 1.8 copy-start.3
  43.1 52.7 %copy-start.8 = (f32[256]{0:T(256)S(1)}, f32[256]{0:T(256)}, u32[]{:S(2)}) copy-start(f32[256]{0:T(256)} %param.22) | copy-start | bytes 3076
  45.2 124.5 %all-gather.8.cloned.1.call-start = ((), (), s32[]{:S(2)}) async-start(), calls=%async_computation.4 | async-start | bytes 1769472 | tf_op jit(solution)/shard_map/all_gather | solution.py:49
  116.3 200.0 %reduce-scatter.2.cloned.1.call-start = ((), (), s32[]{:S(2)}) async-start(), calls=%async_computation.6 | async-start | bytes 2654208 | tf_op jit(solution)/shard_map/reduce_scatter | solution.py:70
  180.1 1.9 copy-start.1
  185.1 1.6 copy-start.2
  232.0 0.7 copy-start.12
  232.0 1.4 copy-start.4
  232.0 1.4 copy-start.6
  232.1 4.7 %copy-start.7 = (bf16[2048,64]{0,1:T(8,128)(2,1)S(1)}, bf16[2048,64]{0,1:T(8,128)(2,1)}, u32[]{:S(2)}) copy-start(bf16[2048,64]{0,1:T(8,128)(2,1)} %param.28) | copy-start | bytes 786436
  232.1 118.1 %all-gather.12.cloned.1.call-start = ((), (), s32[]{:S(2)}) async-start(), calls=%async_computation.7 | async-start | bytes 1769472 | tf_op jit(solution)/shard_map/all_gather | solution.py:43
  233.5 7.0 %copy-start.5 = (bf16[2048,128]{1,0:T(8,128)(2,1)S(1)}, bf16[2048,128]{1,0:T(8,128)(2,1)}, u32[]{:S(2)}) copy-start(bf16[2048,128]{1,0:T(8,128)(2,1)} %param.26) | copy-start | bytes 1572868
  234.1 7.0 %collective-permute-start.1 = (bf16[128,64]{0,1:T(8,128)(2,1)S(1)}, bf16[128,64]{0,1:T(8,128)(2,1)S(1)}, u32[]{:S(2)}, u32[]{:S(2)}) collective-permute-start(bf16[128,64]{0,1:T(8,128)(2,1)S(1)} %slice.51), channel_id=1, source_target_pairs={{0,8},{8,16},{16,24},{24,32},{32,40},{40,48},{48,56},{56,64},{64,7... | collective-permute-start | bytes 49160 | tf_op jit(solution)/shard_map/ppermute | solution.py:80
  237.4 4.6 %collective-permute-start = (bf16[128,64]{0,1:T(8,128)(2,1)S(1)}, bf16[128,64]{0,1:T(8,128)(2,1)S(1)}, u32[]{:S(2)}, u32[]{:S(2)}) collective-permute-start(bf16[128,64]{0,1:T(8,128)(2,1)S(1)} %slice.50), channel_id=1, source_target_pairs={{0,8},{8,16},{16,24},{24,32},{32,40},{40,48},{48,56},{56,64},{64,7... | collective-permute-start | bytes 49160 | tf_op jit(solution)/shard_map/ppermute | solution.py:80
  242.4 107.8 %copy-start.10 = (bf16[1024,256]{1,0:T(8,128)(2,1)S(1)}, bf16[1024,256]{1,0:T(8,128)(2,1)}, u32[]{:S(2)}) copy-start(bf16[1024,256]{1,0:T(8,128)(2,1)} %param.30) | copy-start | bytes 1572868
  318.6 33.3 %copy-start.11 = (bf16[1024,256]{1,0:T(8,128)(2,1)S(1)}, bf16[1024,256]{1,0:T(8,128)(2,1)}, u32[]{:S(2)}) copy-start(bf16[1024,256]{1,0:T(8,128)(2,1)} %param.31) | copy-start | bytes 1572868
  350.2 1.7 copy-start.9
Sparse Core Ops, SparseCore 0:
  10.3 83.8 all-gather.5
  96.3 32.2 all-gather.9
  130.7 38.5 all-gather.7
  232.2 84.0 reduce-scatter.1
  319.5 30.6 all-gather.11
where the time goes:
time: 361 us; the launch traced here: 360 us
  waiting for transfers between devices  174 us (48%)
  blocking collectives  92.2 us (26%)
  local copies, waits for them, and re-layouts  23.2 us (6%)
  matrix products  17.9 us (5%)
  starting transfers between devices  16.4 us (5%)
  other arithmetic  13.6 us (4%)
  between operations  13.5 us (4%)
  loops' own time  8.35 us (2%)
    all_gather x3, waiting for transfers between devices, in_one_piece(): lax.all_gather(both, axis, axis=dim, tiled=True)  79.8 us
    reduce_scatter x1, waiting for transfers between devices, in_one_piece_2(): result = lax.psum_scatter(both, axis, scatter_dimension=dim, tiled=True)  73.9 us
    all_gather x3, blocking collectives, stacked_from(): tiles = lax.all_gather(tiles, axes[k], axis=0, tiled=True)  62.3 us
    all_to_all x1, blocking collectives, copy_for_each(): return lax.all_to_all(copies, axis, split_axis=0, concat_axis=0, tiled=True)  29.9 us
    all_to_all x1, waiting for transfers between devices, copy_for_each(): return lax.all_to_all(copies, axis, split_axis=0, concat_axis=0, tiled=True)  20.6 us
    all_to_all x1, starting transfers between devices, copy_for_each(): return lax.all_to_all(copies, axis, split_axis=0, concat_axis=0, tiled=True)  10.3 us
    another operation x1, loops' own time, attend_latent(): return lax.fori_loop(0, key_count // span_rows, update, state_in)  8.16 us
  transfers between devices with their start and end apart: 8, of which 4 were waited for; matrix products, arithmetic and copies ran while one was open for 6% of the time, Pallas kernels for 0%

commit v1 on v0

--- a/solution.py
+++ b/solution.py
@@ -46,7 +46,16 @@
 def stacked_from(array, axes, turns):
     tiles = array[None]
     for k in turns:
-        tiles = lax.all_gather(tiles, axes[k], axis=0, tiled=True)
+        routes_all_store = lambda x_part, link_axis: jnp.concatenate(
+            lax.all_to_all(
+                jnp.stack(lax.axis_size(link_axis) * [x_part]),
+                axis_name=link_axis,
+                split_axis=0,
+                concat_axis=0,
+            ),
+            0,
+        )
+        tiles = routes_all_store(tiles, axes[k])
     held = [lax.axis_size(axes[k]) for k in reversed(turns)]
     tiles = tiles.reshape(*held, *array.shape)
     turned = sorted(range(len(turns)), key=lambda place: turns[len(turns) - 1 - place])

time: 361 us -> 351 us (0.972)
  blocking collectives: 92.2 us -> 31.4 us
  waiting for transfers between devices: 174 us -> 208 us
  starting transfers between devices: 16.4 us -> 27.2 us
  local copies, waits for them, and re-layouts: 23.2 us -> 27.4 us
    all_gather x3 -> x0, blocking collectives: 62.3 us -> none  [stacked_from(): tiles = lax.all_gather(tiles, axes[k], axis=0, tiled=True)]
    all_to_all x0 -> x3, waiting for transfers between devices: none -> 32.4 us  [stacked_from(): lax.all_to_all(jnp.stack(lax.axis_size(link_axis) * [x_part]), axis_name=...]
    all_to_all x0 -> x1, blocking collectives: none -> 15.1 us  [stacked_from(): lax.all_to_all(jnp.stack(lax.axis_size(link_axis) * [x_part]), axis_name=...]
    all_to_all x1, blocking collectives: 29.9 us -> 16.3 us  [copy_for_each(): return lax.all_to_all(copies, axis, split_axis=0, concat_axis=0, tiled=True)]
    all_to_all x0 -> x3, starting transfers between devices: none -> 12 us  [stacked_from(): lax.all_to_all(jnp.stack(lax.axis_size(link_axis) * [x_part]), axis_name=...]
    all_gather x3, waiting for transfers between devices: 79.8 us -> 85.1 us  [in_one_piece(): lax.all_gather(both, axis, axis=dim, tiled=True)]
    reduce_scatter x1, waiting for transfers between devices: 73.9 us -> 69.9 us  [in_one_piece_2(): result = lax.psum_scatter(both, axis, scatter_dimension=dim, tiled=True)]
  transfers between devices with their start and end apart: 8 -> 10, of which waited for: 4 -> 8; matrix products, arithmetic and copies ran while one was open for 6% -> 6% of each run, Pallas kernels for 0% -> 0%
where the time goes in v1:
time: 351 us; the launch traced here: 350 us
  waiting for transfers between devices  208 us (59%)
  blocking collectives  31.4 us (9%)
  local copies, waits for them, and re-layouts  27.4 us (8%)
  starting transfers between devices  27.2 us (8%)
  matrix products  18.9 us (5%)
  between operations  15.4 us (4%)
  other arithmetic  13.5 us (4%)
  loops' own time  7.9 us (2%)
    all_gather x3, waiting for transfers between devices, in_one_piece(): lax.all_gather(both, axis, axis=dim, tiled=True)  85.1 us
    reduce_scatter x1, waiting for transfers between devices, in_one_piece_2(): result = lax.psum_scatter(both, axis, scatter_dimension=dim, tiled=True)  69.9 us
    all_to_all x3, waiting for transfers between devices, stacked_from(): lax.all_to_all(jnp.stack(lax.axis_size(link_axis) * [x_part]), axis_name=...  32.4 us
    all_to_all x1, waiting for transfers between devices, copy_for_each(): return lax.all_to_all(copies, axis, split_axis=0, concat_axis=0, tiled=True)  20.6 us
    all_to_all x1, blocking collectives, copy_for_each(): return lax.all_to_all(copies, axis, split_axis=0, concat_axis=0, tiled=True)  16.3 us
    all_to_all x1, blocking collectives, stacked_from(): lax.all_to_all(jnp.stack(lax.axis_size(link_axis) * [x_part]), axis_name=...  15.1 us
    all_to_all x3, starting transfers between devices, stacked_from(): lax.all_to_all(jnp.stack(lax.axis_size(link_axis) * [x_part]), axis_name=...  12 us
    all_to_all x1, starting transfers between devices, copy_for_each(): return lax.all_to_all(copies, axis, split_axis=0, concat_axis=0, tiled=True)  10.3 us
  transfers between devices with their start and end apart: 10, of which 8 were waited for; matrix products, arithmetic and copies ran while one was open for 6% of the time, Pallas kernels for 0%

profile of v1, /device:TPU:1, one launch (start us, length us, event | category | flops | bytes accessed | tf_op | source)
XLA Modules:
  0.0 349.6 jit_solution(5283499771203252947)
XLA Ops:
  12.3 10.3 %all-to-all-start.2 = ((bf16[8,48,2048]{2,1,0:T(8,128)(2,1)}), bf16[8,48,2048]{2,1,0:T(8,128)(2,1)S(1)}, u32[]{:S(2)}, u32[]{:S(2)}) async-start(bf16[8,48,2048]{2,1,0:T(8,128)(2,1)} %broadcast_in_dim.63), calls=%async_computation.2 | async-start | bytes 3145728 | tf_op jit(solution)/shard_map/all_to_all | solution.py:30
  22.7 20.6 %all-to-all-done.2 = bf16[8,48,2048]{2,1,0:T(8,128)(2,1)S(1)} async-done(((bf16[8,48,2048]{2,1,0:T(8,128)(2,1)}), bf16[8,48,2048]{2,1,0:T(8,128)(2,1)S(1)}, u32[]{:S(2)}, u32[]{:S(2)}) %all-to-all-start.2) | async-done | bytes 1572896 | tf_op jit(solution)/shard_map/all_to_all | solution.py:30
  45.0 50.0 %all-gather.4.cloned.1.call-done = bf16[2048,320]{1,0:T(8,128)(2,1)} async-done(((bf16[32,320]{1,0:T(8,128)(2,1)}), bf16[2048,320]{1,0:T(8,128)(2,1)}) %all-gather.4.cloned.1.call-update) | async-done | bytes 1310736 | tf_op jit(solution)/shard_map/all_gather | solution.py:43
  95.0 1.5 convolution_convert_fusion.7
  99.0 4.3 %all-to-all-start.3 = ((bf16[8,2,1536]{2,1,0:T(2,128)(2,1)}), bf16[8,2,1536]{2,1,0:T(2,128)(2,1)S(1)}, u32[]{:S(2)}, u32[]{:S(2)}) async-start(bf16[8,2,1536]{2,1,0:T(2,128)(2,1)} %reshape.368), calls=%async_computation.3 | async-start | bytes 98304 | tf_op jit(solution)/shard_map/all_to_all | solution.py:50
  103.4 7.0 %all-to-all-done.3 = bf16[8,2,1536]{2,1,0:T(2,128)(2,1)S(1)} async-done(((bf16[8,2,1536]{2,1,0:T(2,128)(2,1)}), bf16[8,2,1536]{2,1,0:T(2,128)(2,1)S(1)}, u32[]{:S(2)}, u32[]{:S(2)}) %all-to-all-start.3) | async-done | bytes 49184 | tf_op jit(solution)/shard_map/all_to_all | solution.py:50
  111.0 3.4 all-to-all-start
  116.3 6.7 %all-to-all-done = bf16[8,1,48,256]{3,2,1,0:T(8,128)(2,1)S(1)} async-done(((bf16[8,1,48,256]{3,2,1,0:T(8,128)(2,1)}), bf16[8,1,48,256]{3,2,1,0:T(8,128)(2,1)S(1)}, u32[]{:S(2)}, u32[]{:S(2)}) %all-to-all-start) | async-done | bytes 196640 | tf_op jit(solution)/shard_map/all_to_all | solution.py:50
  123.0 15.1 %all_to_all.30 = bf16[8,2,12288]{2,1,0:T(2,128)(2,1)S(1)} all-to-all(bf16[8,2,12288]{2,1,0:T(2,128)(2,1)S(1)} %reshape.370), channel_id=1, replica_groups=mesh['sp_0'=8,'sp_1'=8,'tp'=8] {'sp_1'}, dimensions={0} | all-to-all | bytes 786432 | tf_op jit(solution)/shard_map/all_to_all | solution.py:50
  139.4 4.3 %all-to-all-start.1 = ((bf16[8,8,48,256]{3,2,1,0:T(8,128)(2,1)}), bf16[8,8,48,256]{3,2,1,0:T(8,128)(2,1)}, u32[]{:S(2)}, u32[]{:S(2)}) async-start(bf16[8,8,48,256]{3,2,1,0:T(8,128)(2,1)} %stack.13), calls=%async_computation.1 | async-start | bytes 3145728 | tf_op jit(solution)/shard_map/all_to_all | solution.py:50
  145.1 1.7 copy.37
  146.7 2.0 reshape_reshape.7
  148.8 4.4 %all-gather.6.cloned.1.call-done = bf16[8,384,320]{1,2,0:T(8,128)(2,1)} async-done(((bf16[1,384,320]{1,2,0:T(8,128)(2,1)}), bf16[8,384,320]{1,2,0:T(8,128)(2,1)}) %all-gather.6.cloned.1.call-update) | async-done | bytes 1966096 | tf_op jit(solution)/shard_map/all_gather | solution.py:43
  153.1 2.7 split.33
  155.9 1.7 copy.38
  158.6 18.7 %all-to-all-done.1 = bf16[8,8,48,256]{3,2,1,0:T(8,128)(2,1)} async-done(((bf16[8,8,48,256]{3,2,1,0:T(8,128)(2,1)}), bf16[8,8,48,256]{3,2,1,0:T(8,128)(2,1)}, u32[]{:S(2)}, u32[]{:S(2)}) %all-to-all-start.1) | async-done | bytes 1572896 | tf_op jit(solution)/shard_map/all_to_all | solution.py:50
  177.4 2.8 copy.36
  180.1 1.9 broadcast_in_dim.62
  182.0 22.0 %while.18 = (s32[]{:T(128)}, f32[8,384]{1,0:T(8,128)S(1)}, f32[8,384]{1,0:T(8,128)S(1)}, f32[8,384,256]{2,1,0:T(8,128)}, s32[3072]{0:T(1024)S(1)}, /*index=5*/s3...) while((s32[]{:T(128)}, f32[8,384]{1,0:T(8,128)S(1)}, ...), condition=%wide.region_7.8_spmd.clone, body=%wide.region_2.7_spmd.clone.sunk | while | flops 1829443968 | bytes 66466276 | solution.py:160
  183.9 10.4 %conditional.3 = ((f32[8,384]{1,0:T(8,128)S(1)}, f32[8,384]{1,0:T(8,128)S(1)}, f32[8,384,256]{2,1,0:T(8,128)})) conditional(s32[]{:T(128)} %convert_element_type.208, (f32[8,384]{1,0:T(8,128)S(1)}, f32[8,384]{1,0:T(8,128)S(1)}, f32[8,384,256]{2,1,0:T(8,128)}) %tuple.53, (s32[512]{0:T(512)S(1)}, s32[]{:T(128)}, s32[]{:T(128)}, ...), branch_computations={%region_3.3_spmd, %region_4.6_spmd} | conditional | flops 1829443968 | bytes 66460312 | solution.py:158
  185.1 2.5 fusion.83
  189.6 3.1 multiply_add_fusion
  192.7 1.6 copy-done.2
  204.1 16.3 %all_to_all.31 = f32[8,8,384]{2,1,0:T(8,128)S(1)} all-to-all(f32[8,8,384]{2,1,0:T(8,128)S(1)} %broadcast_in_dim.64), channel_id=1, replica_groups=mesh['sp_0'=8,'sp_1'=8,'tp'=8] {'tp'}, dimensions={0} | all-to-all | bytes 196608 | tf_op jit(solution)/shard_map/all_to_all | solution.py:30
  220.8 2.4 multiply_convert_fusion
  223.2 2.5 pad_maximum_fusion
  227.7 1.8 collective-permute-start.1
  230.2 2.5 collective-permute-start
  234.5 69.9 %reduce-scatter.2.cloned.1.call-done = bf16[1,384,257]{2,1,0:T(8,128)(2,1)} async-done(((bf16[8,384,257]{2,1,0:T(8,128)(2,1)}), bf16[1,384,257]{2,1,0:T(8,128)(2,1)}) %reduce-scatter.2.cloned.1.call-update) | async-done | bytes 197392 | tf_op jit(solution)/shard_map/reduce_scatter | solution.py:79
  307.5 30.7 %all-gather.8.cloned.1.call-done = bf16[768,1024]{0,1:T(8,128)(2,1)} async-done(((bf16[768,128]{0,1:T(8,128)(2,1)}), bf16[768,1024]{0,1:T(8,128)(2,1)}) %all-gather.8.cloned.1.call-update) | async-done | bytes 1572880 | tf_op jit(solution)/shard_map/all_gather | solution.py:43
  338.2 1.7 fusion.29
  339.9 2.1 fusion.23
  (119 shorter events, 30.3 us)
Async XLA Ops:
  7.4 35.9 %copy-start = (bf16[2048,192]{0,1:T(8,128)(2,1)S(1)}, bf16[2048,192]{0,1:T(8,128)(2,1)}, u32[]{:S(2)}) copy-start(bf16[2048,192]{0,1:T(8,128)(2,1)} %param.23) | copy-start | bytes 2359300
  7.4 87.7 %all-gather.4.cloned.1.call-start = ((), (), s32[]{:S(2)}) async-start(), calls=%async_computation.7 | async-start | bytes 1597440 | tf_op jit(solution)/shard_map/all_gather | solution.py:43
  12.3 30.9 %all-to-all-start.2 = ((bf16[8,48,2048]{2,1,0:T(8,128)(2,1)}), bf16[8,48,2048]{2,1,0:T(8,128)(2,1)S(1)}, u32[]{:S(2)}, u32[]{:S(2)}) async-start(bf16[8,48,2048]{2,1,0:T(8,128)(2,1)} %broadcast_in_dim.63), calls=%async_computation.2 | async-start | bytes 3145728 | tf_op jit(solution)/shard_map/all_to_all | solution.py:30
  43.3 1.8 copy-start.3
  43.9 59.4 %copy-start.8 = (f32[256]{0:T(256)S(1)}, f32[256]{0:T(256)}, u32[]{:S(2)}) copy-start(f32[256]{0:T(256)} %param.22) | copy-start | bytes 3076
  99.0 11.4 %all-to-all-start.3 = ((bf16[8,2,1536]{2,1,0:T(2,128)(2,1)}), bf16[8,2,1536]{2,1,0:T(2,128)(2,1)S(1)}, u32[]{:S(2)}, u32[]{:S(2)}) async-start(bf16[8,2,1536]{2,1,0:T(2,128)(2,1)} %reshape.368), calls=%async_computation.3 | async-start | bytes 98304 | tf_op jit(solution)/shard_map/all_to_all | solution.py:50
  111.0 11.9 %all-to-all-start = ((bf16[8,1,48,256]{3,2,1,0:T(8,128)(2,1)}), bf16[8,1,48,256]{3,2,1,0:T(8,128)(2,1)S(1)}, u32[]{:S(2)}, u32[]{:S(2)}) async-start(bf16[8,1,48,256]{3,2,1,0:T(8,128)(2,1)} %stack.12), calls=%async_computation | async-start | bytes 393216 | tf_op jit(solution)/shard_map/all_to_all | solution.py:50
  114.4 38.7 %all-gather.6.cloned.1.call-start = ((), (), s32[]{:S(2)}) async-start(), calls=%async_computation.8 | async-start | bytes 2211840 | tf_op jit(solution)/shard_map/all_gather | solution.py:43
  139.4 38.0 %all-to-all-start.1 = ((bf16[8,8,48,256]{3,2,1,0:T(8,128)(2,1)}), bf16[8,8,48,256]{3,2,1,0:T(8,128)(2,1)}, u32[]{:S(2)}, u32[]{:S(2)}) async-start(bf16[8,8,48,256]{3,2,1,0:T(8,128)(2,1)} %stack.13), calls=%async_computation.1 | async-start | bytes 3145728 | tf_op jit(solution)/shard_map/all_to_all | solution.py:50
  143.7 160.7 %reduce-scatter.2.cloned.1.call-start = ((), (), s32[]{:S(2)}) async-start(), calls=%async_computation.9 | async-start | bytes 2654208 | tf_op jit(solution)/shard_map/reduce_scatter | solution.py:79
  187.7 1.9 copy-start.1
  192.7 1.7 copy-start.2
  225.7 0.7 copy-start.11
  225.7 1.4 copy-start.4
  225.7 1.4 copy-start.6
  225.7 3.9 %copy-start.7 = (bf16[2048,64]{0,1:T(8,128)(2,1)S(1)}, bf16[2048,64]{0,1:T(8,128)(2,1)}, u32[]{:S(2)}) copy-start(bf16[2048,64]{0,1:T(8,128)(2,1)} %param.28) | copy-start | bytes 786436
  225.7 112.5 %all-gather.8.cloned.1.call-start = ((), (), s32[]{:S(2)}) async-start(), calls=%async_computation.10 | async-start | bytes 1769472 | tf_op jit(solution)/shard_map/all_gather | solution.py:43
  227.1 5.5 %copy-start.5 = (bf16[2048,128]{1,0:T(8,128)(2,1)S(1)}, bf16[2048,128]{1,0:T(8,128)(2,1)}, u32[]{:S(2)}) copy-start(bf16[2048,128]{1,0:T(8,128)(2,1)} %param.26) | copy-start | bytes 1572868
  227.7 5.5 %collective-permute-start.1 = (bf16[128,64]{0,1:T(8,128)(2,1)S(1)}, bf16[128,64]{0,1:T(8,128)(2,1)S(1)}, u32[]{:S(2)}, u32[]{:S(2)}) collective-permute-start(bf16[128,64]{0,1:T(8,128)(2,1)S(1)} %slice.51), channel_id=1, source_target_pairs={{0,8},{8,16},{16,24},{24,32},{32,40},{40,48},{48,56},{56,64},{64,7... | collective-permute-start | bytes 49160 | tf_op jit(solution)/shard_map/ppermute | solution.py:89
  230.2 3.9 %collective-permute-start = (bf16[128,64]{0,1:T(8,128)(2,1)S(1)}, bf16[128,64]{0,1:T(8,128)(2,1)S(1)}, u32[]{:S(2)}, u32[]{:S(2)}) collective-permute-start(bf16[128,64]{0,1:T(8,128)(2,1)S(1)} %slice.50), channel_id=1, source_target_pairs={{0,8},{8,16},{16,24},{24,32},{32,40},{40,48},{48,56},{56,64},{64,7... | collective-permute-start | bytes 49160 | tf_op jit(solution)/shard_map/ppermute | solution.py:89
  234.5 103.7 %copy-start.10 = (bf16[1024,256]{1,0:T(8,128)(2,1)S(1)}, bf16[1024,256]{1,0:T(8,128)(2,1)}, u32[]{:S(2)}) copy-start(bf16[1024,256]{1,0:T(8,128)(2,1)} %param.30) | copy-start | bytes 1572868
  338.2 1.7 copy-start.9
Sparse Core Ops, SparseCore 0:
  11.2 83.8 all-gather.3
Sparse Core Ops, SparseCore 1:
  117.0 36.0 all-gather.5
  225.8 78.6 reduce-scatter.1
  307.6 30.5 all-gather.7
